TPU v7x, 128 devices: a whole 4x4x4 slice. The times are simulated.
128 devices in a mesh: ep: 64 (over z, y, x), tp: 2 (over core).
Axes of the slice: x: 4, y: 4, z: 4, core: 2. Of those that a mesh axis runs over, the one named last changes fastest.
Arguments:
- hidden_in: bfloat16 [2048, 2048], P('ep'), may hold values from -6 to 6
- past_lengths: int32 [2048], P('ep'), may hold values from 1 to 1023, as said below
- key_cache: bfloat16 [2048, 1024, 256], P('ep', None, 'tp'), may hold values from -512 to 512
- value_cache: bfloat16 [2048, 1024, 256], P('ep', None, 'tp'), may hold values from -6 to 6
- attn_gain: float32 [2048], replicated, may hold values from 0.1 to 1.9
- w_query: bfloat16 [2048, 2048], P(None, 'tp'), may hold values from -0.125 to 0.125
- w_key: bfloat16 [2048, 256], P(None, 'tp'), may hold values from -0.125 to 0.125
- w_value: bfloat16 [2048, 256], P(None, 'tp'), may hold values from -0.125 to 0.125
- lambdas: float32 [16], P('tp'), may hold values from 0.3 to 0.8
- head_gain: float32 [128], replicated, may hold values from 0.1 to 1.9
- w_out: bfloat16 [2048, 2048], P('tp'), may hold values from -0.125 to 0.125
- ffn_gain: float32 [2048], replicated, may hold values from 0.1 to 1.9
- route_ids: int32 [2048, 2], P('ep'), may hold values from 0 to 31, all different within a row; in each aligned block of 32 rows (0 to 31, 32 to 63, ...) at most 4 rows name the same one
- route_weights: float32 [2048, 2], P('ep'), may hold values from 0.2 to 1
- expert_gate: bfloat16 [64, 2048, 704], P('ep', None, 'tp'), may hold values from -0.125 to 0.125
- expert_up: bfloat16 [64, 2048, 704], P('ep', None, 'tp'), may hold values from -0.125 to 0.125
- expert_down: bfloat16 [64, 704, 2048], P('ep', None, 'tp'), may hold values from -1.25 to 1.25
- gate_vector: bfloat16 [2048], replicated, may hold values from -0.125 to 0.125
- dense_gate: bfloat16 [2048, 5632], P(None, ('ep', 'tp')), may hold values from -0.125 to 0.125
- dense_up: bfloat16 [2048, 5632], P(None, ('ep', 'tp')), may hold values from -0.125 to 0.125
- dense_down: bfloat16 [5632, 2048], P('ep', 'tp'), may hold values from -0.625 to 0.625
Outputs:
- mixed_out: bfloat16 [2048, 2048], P('ep', 'tp')
- new_keys: bfloat16 [2048, 256], P('ep', 'tp')
- new_values: bfloat16 [2048, 256], P('ep', 'tp')
Inputs may be any that keep to these rules, and one draw needn't show every extreme that they name: `past_lengths`: the new token of a sequence stands at this position; some sequence has 1023 cached positions in every draw. `route_ids`: each row names 2 different experts; among the rows of one index of ep no expert is named more than 4 times, a bound that some block reaches in every draw.
All inputs are finite; a program needn't handle non-finite values.
Results may differ from a plain program's by a relative error of at most 0.02.
The roundings to bfloat16 on the way count: a program that leaves them out, or rounds other values in their place, can miss the bound.
Values may be sent and summed in bfloat16 or wider, within the bound.
A program may use at most 128 MiB of HBM per device.

v0:
```python
import jax
import jax.numpy as jnp
from jax import lax
from jax.sharding import PartitionSpec as P

HEAD_DIM = 64
VALUE_DIM = 128
norm_eps = 1e-05
rope_base = 10000.0


def sent_to_all(x, axis):
    size = lax.axis_size(axis)
    return lax.all_to_all(jnp.broadcast_to(x[None], (size, *x.shape)), axis, 0, 0, tiled=True)


def taken_together(x, axis):
    return sent_to_all(x, axis).astype(jnp.float32).sum(axis=0)


def in_order(pieces, dim):
    pieces = jnp.moveaxis(pieces, 0, dim)
    shape = pieces.shape
    return pieces.reshape(*shape[:dim], shape[dim] * shape[dim + 1], *shape[dim + 2 :])


def collect(x, axis, dim):
    pieces = sent_to_all(x, axis)
    return in_order(pieces, dim)


def in_one_piece(arrays, axis, dim, along):
    columns = [a.reshape(*a.shape[:along], -1) for a in arrays]
    both = jnp.concatenate(columns, axis=along)
    filled, at, outs = (lax.all_gather(both, axis, axis=dim, tiled=True), 0, [])
    for a, column in zip(arrays, columns):
        piece = filled[..., at : at + column.shape[along]]
        outs.append(piece.reshape(*piece.shape[:along], *a.shape[along:]))
        at += column.shape[along]
    return tuple(outs)


def side_by_side(arrays, axis, split_dim, concat_dim, along):
    both = jnp.concatenate(arrays, axis=along)
    filled, at, outs = (
        lax.all_to_all(both, axis, split_axis=split_dim, concat_axis=concat_dim, tiled=True),
        0,
        [],
    )
    for a in arrays:
        outs.append(lax.slice_in_dim(filled, at, at + a.shape[along], axis=along))
        at += a.shape[along]
    return tuple(outs)


def cut_along(x, dim, size):
    shape = x.shape
    pieces = x.reshape(*shape[:dim], size, shape[dim] // size, *shape[dim + 1 :])
    return jnp.moveaxis(pieces, dim, 0)


def sum_at_owner(x, axis, dim):
    pieces = cut_along(x, dim, lax.axis_size(axis))
    arrived = lax.all_to_all(pieces, axis, split_axis=0, concat_axis=0, tiled=True)
    return arrived.astype(jnp.float32).sum(axis=0)


def rms_rows(values, scales):
    values = values.astype(jnp.float32)
    return values * lax.rsqrt(jnp.mean(values * values, axis=-1, keepdims=True) + norm_eps) * scales


def rotary(values, position):
    middle = values.shape[-1] // 2
    inverse = rope_base ** (-jnp.arange(middle, dtype=jnp.float32) / middle)
    angles = position.astype(jnp.float32)[:, None] * inverse[None, :]
    cosine = jnp.cos(angles)[:, None, None, :]
    sine_part = jnp.sin(angles)[:, None, None, :]
    leading, second = (values[..., :middle], values[..., middle:])
    return jnp.concatenate(
        [leading * cosine - second * sine_part, second * cosine + leading * sine_part], axis=-1
    )


def per_device(
    hidden_in,
    past_lengths,
    key_cache,
    value_cache,
    attn_gain,
    w_query,
    w_key,
    w_value,
    lambdas,
    head_gain,
    w_out,
    ffn_gain,
    route_ids,
    route_weights,
    expert_gate,
    expert_up,
    expert_down,
    gate_vector,
    dense_gate,
    dense_up,
    dense_down,
):
    batch_rows = hidden_in.shape[0]
    model_width = hidden_in.shape[1]
    tp_count = lax.axis_size("tp")
    ep_count = lax.axis_size("ep")
    tp_rank = lax.axis_index("tp")
    half_width = model_width // tp_count
    heads_here = lambdas.shape[0]
    kv_here = w_key.shape[1] // (2 * HEAD_DIM)
    per_key = heads_here // kv_here
    scale_qk = HEAD_DIM ** (-0.5)
    normed = rms_rows(hidden_in, attn_gain).astype(jnp.bfloat16)
    queries = rotary(
        jnp.dot(normed, w_query, preferred_element_type=jnp.float32).reshape(
            batch_rows, heads_here, 2, HEAD_DIM
        ),
        past_lengths,
    ).astype(jnp.bfloat16)
    key_new = rotary(
        jnp.dot(normed, w_key, preferred_element_type=jnp.float32).reshape(
            batch_rows, kv_here, 2, HEAD_DIM
        ),
        past_lengths,
    ).astype(jnp.bfloat16)
    value_new = jnp.dot(normed, w_value, preferred_element_type=jnp.float32).astype(jnp.bfloat16)
    grouped = queries.reshape(batch_rows, kv_here, per_key, 2, HEAD_DIM)
    own_score = (
        jnp.einsum("sgamd,sgmd->sgam", grouped, key_new, preferred_element_type=jnp.float32)
        * scale_qk
    )
    value_rows = value_new.reshape(batch_rows, kv_here, 1, 1, VALUE_DIM).astype(jnp.float32)
    start_state = (
        own_score,
        jnp.ones_like(own_score),
        jnp.broadcast_to(value_rows, own_score.shape + (VALUE_DIM,)),
    )
    cache_len = key_cache.shape[1]
    span_len = min(256, cache_len)
    spans_needed = (jnp.max(past_lengths) + span_len - 1) // span_len

    def visit(block_index, carried):
        running, totals, summed = carried
        offset = block_index * span_len
        key_rows = lax.dynamic_slice_in_dim(key_cache, offset, span_len, 1).reshape(
            batch_rows, span_len, kv_here, 2, HEAD_DIM
        )
        cached = lax.dynamic_slice_in_dim(value_cache, offset, span_len, 1).reshape(
            batch_rows, span_len, kv_here, VALUE_DIM
        )
        scores = (
            jnp.einsum("sgamd,slgmd->sgaml", grouped, key_rows, preferred_element_type=jnp.float32)
            * scale_qk
        )
        usable = (offset + jnp.arange(span_len))[None, :] < past_lengths[:, None]
        scores = jnp.where(usable[:, None, None, None, :], scores, -jnp.inf)
        raised = jnp.maximum(running, jnp.max(scores, axis=-1))
        fading = jnp.exp(running - raised)
        weights = jnp.exp(scores - raised[..., None])
        totals = totals * fading + jnp.sum(weights, axis=-1)
        summed = summed * fading[..., None] + jnp.einsum(
            "sgaml,slge->sgame",
            weights.astype(jnp.bfloat16),
            cached,
            preferred_element_type=jnp.float32,
        )
        return (raised, totals, summed)

    running, totals, summed = lax.fori_loop(0, spans_needed, visit, start_state)
    mapped = summed / totals[..., None]
    head_mix = mapped[..., 0, :] - lambdas.reshape(1, kv_here, per_key, 1) * mapped[..., 1, :]
    head_out = rms_rows(head_mix, head_gain).astype(jnp.bfloat16).reshape(batch_rows, -1)
    attn_out = (
        taken_together(
            jnp.dot(head_out, w_out, preferred_element_type=jnp.float32).astype(jnp.bfloat16), "tp"
        )
        .astype(jnp.float32)
        .astype(jnp.bfloat16)
    )
    residual = hidden_in.astype(jnp.float32) + attn_out.astype(jnp.float32)
    moe_in = rms_rows(residual, ffn_gain).astype(jnp.bfloat16)
    mix_gate = jax.nn.sigmoid(
        jnp.dot(moe_in, gate_vector, preferred_element_type=jnp.float32)
    ).astype(jnp.bfloat16)
    top_count = route_ids.shape[1]
    experts = ep_count // 2
    capacity = max(2, 2 * batch_rows * top_count // experts)
    flat_ids = route_ids.reshape(-1)
    matches = (flat_ids[:, None] == jnp.arange(experts)[None, :]).astype(jnp.int32)
    earlier = jnp.sum((jnp.cumsum(matches, axis=0) - matches) * matches, axis=1)
    slot_of = flat_ids * capacity + earlier
    placing = (jnp.arange(experts * capacity)[:, None] == slot_of[None, :]).astype(jnp.float32)
    repeated = jnp.repeat(moe_in, top_count, axis=0)
    packed = jnp.dot(
        placing.astype(jnp.bfloat16), repeated, preferred_element_type=jnp.float32
    ).astype(jnp.bfloat16)
    outgoing = jnp.broadcast_to(
        packed.reshape(experts, 1, capacity, model_width), (experts, 2, capacity, model_width)
    ).reshape(ep_count, capacity, model_width)
    arrived = lax.all_to_all(outgoing, "ep", split_axis=0, concat_axis=0, tiled=True)
    leading = arrived.shape[:2]
    flat_rows = arrived.reshape(-1, model_width)
    gate_pre = jnp.dot(flat_rows, expert_gate[0], preferred_element_type=jnp.float32)
    up_pre = jnp.dot(flat_rows, expert_up[0], preferred_element_type=jnp.float32)
    inner_act = (jax.nn.silu(gate_pre) * up_pre).astype(jnp.bfloat16)
    inner_act = collect(inner_act, "tp", 1)
    partial_value = jnp.dot(inner_act, expert_down[0], preferred_element_type=jnp.float32).reshape(
        leading + (half_width,)
    )
    returned = lax.all_to_all(
        partial_value.astype(jnp.bfloat16), "ep", split_axis=0, concat_axis=0, tiled=True
    ).astype(partial_value.dtype)
    paired = jnp.sum(returned.reshape(experts, 2, capacity, half_width), axis=1).reshape(
        experts * capacity, half_width
    )
    weighted = (
        (placing * route_weights.reshape(1, -1))
        .reshape(experts * capacity, batch_rows, top_count)
        .sum(axis=2)
    )
    moe_out = jnp.einsum("ct,cd->td", weighted, paired, precision=lax.Precision.HIGHEST)
    own_half = lax.dynamic_slice_in_dim(moe_in, tp_rank * half_width, half_width, 1)
    rows_all, gates_all = in_one_piece((own_half, mix_gate), "ep", 0, 1)
    columns = dense_gate.shape[1]
    gate_cols, up_cols = side_by_side(
        (
            dense_gate.reshape(tp_count, half_width, columns),
            dense_up.reshape(tp_count, half_width, columns),
        ),
        "tp",
        0,
        2,
        1,
    )
    pre_gate, pre_up = (
        taken_together(
            jnp.dot(rows_all, gate_cols[0], preferred_element_type=jnp.float32).astype(
                jnp.bfloat16
            ),
            "tp",
        ).astype(jnp.float32),
        taken_together(
            jnp.dot(rows_all, up_cols[0], preferred_element_type=jnp.float32).astype(jnp.bfloat16),
            "tp",
        ).astype(jnp.float32),
    )
    dense_act = (jax.nn.silu(pre_gate) * pre_up).astype(jnp.bfloat16)
    gate_rows = gates_all.astype(jnp.float32)
    dense_out = sum_at_owner(
        (
            jnp.dot(dense_act, dense_down, preferred_element_type=jnp.float32) * gate_rows[:, None]
        ).astype(jnp.bfloat16),
        "ep",
        0,
    )
    own_residual = lax.dynamic_slice_in_dim(residual, tp_rank * half_width, half_width, 1)
    mixed_out = (own_residual + moe_out + dense_out).astype(jnp.bfloat16)
    return (mixed_out, key_new.reshape(batch_rows, -1), value_new)


def solution(mesh):
    return jax.shard_map(
        per_device,
        mesh=mesh,
        in_specs=(
            P("ep", None),
            P("ep"),
            P("ep", None, "tp"),
            P("ep", None, "tp"),
            P(),
            P(None, "tp"),
            P(None, "tp"),
            P(None, "tp"),
            P("tp"),
            P(),
            P("tp", None),
            P(),
            P("ep", None),
            P("ep", None),
            P("ep", None, "tp"),
            P("ep", None, "tp"),
            P("ep", None, "tp"),
            P(),
            P(None, ("ep", "tp")),
            P(None, ("ep", "tp")),
            P("ep", "tp"),
        ),
        out_specs=(P("ep", "tp"), P("ep", "tp"), P("ep", "tp")),
        check_vma=False,
    )
```

profile of v0, /device:TPU:0, one launch (start us, length us, event | category | flops | bytes accessed | tf_op | source)
XLA Modules:
  0.0 275.6 jit_solution(12817063429684109780)
XLA Ops:
  7.2 1.5 fusion.80
  10.4 3.2 %fusion.73 = f32[32,1024]{1,0:T(8,128)S(1)} fusion(bf16[2048,1024]{1,0:T(8,128)(2,1)} %param.28, bf16[32,2048]{1,0:T(8,128)(2,1)} %param.23, f32[2048]{0:T(1024)} %param.27, f32[32]{0:T(128)S(1)} %add_rsqrt_fusion.2), kind=kOutput, calls=%fused_computation.116 | convolution fusion | flops 134479872 | bytes 4464768 | tf_op jit(solution)/shard_map/dot_general | solution.py:120
  18.3 14.5 %while.14 = (s32[]{:T(128)}, f32[32,1,8,2]{2,3,0,1:T(2,128)}, f32[32,1,8,2]{2,3,0,1:T(2,128)}, f32[32,1,8,2,128]{4,2,3,0,1:T(8,128)}, s32[]{:T(128)}, /*index=5*...) while((s32[]{:T(128)}, f32[32,1,8,2]{2,3,0,1:T(2,128)}, ...), condition=%wide.region_5.6_spmd, body=%wide.region_2.5_spmd.sunk | while | flops 51390212 | bytes 14797119 | solution.py:174
  18.3 3.1 %constant_dynamic-slice_fusion.3 = bf16[32,256,128]{2,1,0:T(8,128)(2,1)} fusion(bf16[32,1024,128]{2,1,0:T(8,128)(2,1)} %get-tuple-element.251, s32[]{:T(128)S(6)} %select_n.26), kind=kLoop, calls=%fused_computation.22.clone.1 | loop fusion | bytes 4194308 | tf_op jit(solution)/shard_map/while/body/dynamic_slice | solution.py:150
  21.4 3.3 %copy.152 = bf16[32,256,128]{1,2,0:T(8,128)(2,1)S(1)} copy(bf16[32,256,128]{2,1,0:T(8,128)(2,1)} %constant_dynamic-slice_fusion.3) | data formatting | bytes 4194304 | tf_op jit(solution)/shard_map/while/body/dynamic_slice | solution.py:150
  25.4 1.4 fusion.104
  27.9 1.4 bitcast_add_fusion.2
  30.0 2.8 %fusion.107 = f32[32,1,8,2,128]{4,2,3,0,1:T(8,128)} fusion(bf16[32,1024,128]{2,1,0:T(8,128)(2,1)} %get-tuple-element.253, s32[]{:T(128)S(6)} %select_n.26, f32[32,1,8,2,256]{4,2,3,0,1:T(8,128)S(1)} %get-tuple-element.217, f32[32,1,8,2,128]{4,2,3,0,1:T(8,128)} %get-tuple-element.235, f32[32,8,2]{1,2,0:T(2,128)S(1)} %bitcast.179, ...), kind=kOutput, calls=%fused_computation.8.clone.1 | convolution fusion | flops 33947648 | bytes 3149828 | tf_op jit(solution)/shard_map/while/body/sgaml,slge->sgame/dot_general | solution.py:166
  32.7 1.1 broadcast_divide_fusion
  35.7 3.0 %convolution_convert_fusion.1 = bf16[32,2048]{1,0:T(8,128)(2,1)S(1)} fusion(bf16[1024,2048]{1,0:T(8,128)(2,1)} %param.33, f32[4,8,8,128]{3,2,1,0:T(8,128)S(1)} %bitcast.186, f32[4,8,8,128]{3,2,1,0:T(8,128)S(1)} %bitcast.188, f32[4,8,8,128]{3,2,1,0:T(8,128)S(1)} %bitcast.187, f32[1024]{0:T(1024)S(1)} %get-tuple-element.153, f32[1024]{0:T(1024)S(1)} %get-tuple-element.154), kind=kOutput, calls=%fused_computation.32 | convolution fusion | flops 134447104 | bytes 4726784 | tf_op jit(solution)/shard_map/dot_general | solution.py:180
  39.4 3.4 %all-to-all-start = ((bf16[2,32,2048]{2,1,0:T(8,128)(2,1)}), bf16[2,32,2048]{2,1,0:T(8,128)(2,1)S(1)}, u32[]{:S(2)}, u32[]{:S(2)}) async-start(bf16[2,32,2048]{2,1,0:T(8,128)(2,1)} %broadcast_in_dim.37), calls=%async_computation | async-start | bytes 524288 | tf_op jit(solution)/shard_map/all_to_all | solution.py:14
  42.9 1.5 all-to-all-done
  47.5 3.5 %all-to-all-start.4 = ((bf16[2,2048,44]{1,2,0:T(8,128)(2,1)}), bf16[2,2048,44]{1,2,0:T(8,128)(2,1)S(1)}, u32[]{:S(2)}, u32[]{:S(2)}) async-start(bf16[2,2048,44]{1,2,0:T(8,128)(2,1)} %pad_maximum_fusion), calls=%async_computation.4 | async-start | bytes 786432 | tf_op jit(solution)/shard_map/all_to_all | solution.py:46
  52.9 1.6 broadcast_in_dim.40
  54.5 54.6 %all-to-all-start.1 = ((bf16[64,4,2048]{2,1,0:T(4,128)(2,1)}), bf16[64,4,2048]{2,1,0:T(4,128)(2,1)S(1)}, u32[]{:S(2)}, u32[]{:S(2)}) async-start(bf16[64,4,2048]{2,1,0:T(4,128)(2,1)} %bitcast.26), calls=%async_computation.1 | async-start | bytes 2097152 | tf_op jit(solution)/shard_map/all_to_all | solution.py:205
  109.9 18.8 %all-to-all-done.1 = bf16[64,4,2048]{2,1,0:T(4,128)(2,1)S(1)} async-done(((bf16[64,4,2048]{2,1,0:T(4,128)(2,1)}), bf16[64,4,2048]{2,1,0:T(4,128)(2,1)S(1)}, u32[]{:S(2)}, u32[]{:S(2)}) %all-to-all-start.1) | async-done | bytes 1048608 | tf_op jit(solution)/shard_map/all_to_all | solution.py:205
  129.0 1.9 fusion.34
  131.0 1.9 fusion.42
  132.9 4.1 %all_to_all.53 = bf16[2,256,352]{1,2,0:T(8,128)(2,1)S(1)} all-to-all(bf16[2,256,352]{1,2,0:T(8,128)(2,1)S(1)} %broadcast_in_dim.41), channel_id=1, replica_groups=mesh['ep'=64,'tp'=2] {'tp'}, dimensions={0} | all-to-all | bytes 720896 | tf_op jit(solution)/shard_map/all_to_all | solution.py:14
  138.6 1.2 copy.120
  139.8 28.0 %all-gather.2.cloned.1.call-done = bf16[2048,1025]{1,0:T(8,128)(2,1)} async-done(((bf16[32,1025]{1,0:T(8,128)(2,1)}), bf16[2048,1025]{1,0:T(8,128)(2,1)}) %all-gather.2.cloned.1.call-update) | async-done | bytes 4198416 | tf_op jit(solution)/shard_map/all_gather | solution.py:35
  167.7 3.6 %fusion.27 = bf16[2048,88]{0,1:T(8,128)(2,1)S(1)} fusion(bf16[2048,1025]{1,0:T(8,128)(2,1)} %all-gather.2.cloned.1.call-done, bf16[1,2048,88]{1,2,0:T(8,128)(2,1)S(1)} %copy-done.6), kind=kOutput, calls=%fused_computation.31 | convolution fusion | flops 369278976 | bytes 4734976 | tf_op jit(solution)/shard_map/dot_general | solution.py:248
  172.3 3.7 %all-to-all-start.6 = ((bf16[2,2048,88]{1,2,0:T(8,128)(2,1)}), bf16[2,2048,88]{1,2,0:T(8,128)(2,1)S(1)}, u32[]{:S(2)}, u32[]{:S(2)}) async-start(bf16[2,2048,88]{1,2,0:T(8,128)(2,1)} %broadcast_in_dim.43), calls=%async_computation.6 | async-start | bytes 1441792 | tf_op jit(solution)/shard_map/all_to_all | solution.py:14
  176.0 3.6 %fusion.24 = bf16[2048,88]{0,1:T(8,128)(2,1)S(1)} fusion(bf16[2048,1025]{1,0:T(8,128)(2,1)} %all-gather.2.cloned.1.call-done, bf16[1,2048,88]{1,2,0:T(8,128)(2,1)S(1)} %copy-done.6), kind=kOutput, calls=%fused_computation.30 | convolution fusion | flops 369278976 | bytes 4734976 | tf_op jit(solution)/shard_map/dot_general | solution.py:242
  180.6 3.5 %all-to-all-start.5 = ((bf16[2,2048,88]{1,2,0:T(8,128)(2,1)}), bf16[2,2048,88]{1,2,0:T(8,128)(2,1)S(1)}, u32[]{:S(2)}, u32[]{:S(2)}) async-start(bf16[2,2048,88]{1,2,0:T(8,128)(2,1)} %broadcast_in_dim.42), calls=%async_computation.5 | async-start | bytes 1441792 | tf_op jit(solution)/shard_map/all_to_all | solution.py:14
  186.0 6.5 %all-to-all-start.3 = ((bf16[64,4,1024]{2,1,0:T(4,128)(2,1)}), bf16[64,4,1024]{2,1,0:T(4,128)(2,1)S(1)}, u32[]{:S(2)}, u32[]{:S(2)}) async-start(bf16[64,4,1024]{2,1,0:T(4,128)(2,1)} %copy.120), calls=%async_computation.3 | async-start | bytes 1048576 | tf_op jit(solution)/shard_map/all_to_all | solution.py:215
  192.6 1.3 convert_reduce_fusion.4
  193.9 4.4 %multiply_convert_fusion = bf16[2048,1024]{1,0:T(8,128)(2,1)} fusion(bf16[88,1024]{1,0:T(8,128)(2,1)S(1)} %copy-done.20, f32[2048]{0:T(1024)S(1)} %convert_reduce_fusion.4, f32[2048,88]{0,1:T(8,128)} %convert_reduce_fusion.1, f32[2048,88]{0,1:T(8,128)S(1)} %convert_reduce_fusion.2), kind=kOutput, calls=%fused_computation.24 | convolution fusion | flops 374374400 | bytes 5824512 | tf_op jit(solution)/shard_map/dot_general | solution.py:256
  198.3 7.9 %all-to-all-done.3 = bf16[64,4,1024]{2,1,0:T(4,128)(2,1)S(1)} async-done(((bf16[64,4,1024]{2,1,0:T(4,128)(2,1)}), bf16[64,4,1024]{2,1,0:T(4,128)(2,1)S(1)}, u32[]{:S(2)}, u32[]{:S(2)}) %all-to-all-start.3) | async-done | bytes 524320 | tf_op jit(solution)/shard_map/all_to_all | solution.py:215
  206.2 5.8 %all-to-all-start.7 = ((bf16[64,32,1024]{2,1,0:T(8,128)(2,1)}), bf16[64,32,1024]{2,1,0:T(8,128)(2,1)}, u32[]{:S(2)}, u32[]{:S(2)}) async-start(bf16[64,32,1024]{2,1,0:T(8,128)(2,1)} %bitcast.180), calls=%async_computation.7 | async-start | bytes 8388608 | tf_op jit(solution)/shard_map/all_to_all | solution.py:64
  213.6 51.1 %all-to-all-done.7 = bf16[64,32,1024]{2,1,0:T(8,128)(2,1)} async-done(((bf16[64,32,1024]{2,1,0:T(8,128)(2,1)}), bf16[64,32,1024]{2,1,0:T(8,128)(2,1)}, u32[]{:S(2)}, u32[]{:S(2)}) %all-to-all-start.7) | async-done | bytes 4194336 | tf_op jit(solution)/shard_map/all_to_all | solution.py:64
  264.7 3.0 %convert_reduce_fusion = f32[32,1024]{1,0:T(8,128)S(1)} fusion(bf16[64,32,1024]{2,1,0:T(8,128)(2,1)} %all-to-all-done.7), kind=kLoop, calls=%fused_computation.23 | loop fusion | flops 4161536 | bytes 4325376 | tf_op jit(solution)/shard_map/reduce_sum | solution.py:65
  (118 shorter events, 24.5 us)
Async XLA Ops:
  7.2 130.8 %copy-start = (bf16[1,704,1024]{2,1,0:T(8,128)(2,1)S(1)}, bf16[1,704,1024]{2,1,0:T(8,128)(2,1)}, u32[]{:S(2)}) copy-start(bf16[1,704,1024]{2,1,0:T(8,128)(2,1)} %param.39) | copy-start | bytes 4325380
  7.2 6.9 %copy-start.1 = (bf16[32,2048]{1,0:T(8,128)(2,1)S(1)}, bf16[32,2048]{1,0:T(8,128)(2,1)}, u32[]{:S(2)}) copy-start(bf16[32,2048]{1,0:T(8,128)(2,1)} %param.23) | copy-start | bytes 393220
  7.2 6.9 %copy-start.11 = (f32[2048]{0:T(1024)S(1)}, f32[2048]{0:T(1024)}, u32[]{:S(2)}) copy-start(f32[2048]{0:T(1024)} %param.27) | copy-start | bytes 24580
  7.2 6.9 %copy-start.4 = (bf16[2048,128]{1,0:T(8,128)(2,1)S(1)}, bf16[2048,128]{1,0:T(8,128)(2,1)}, u32[]{:S(2)}) copy-start(bf16[2048,128]{1,0:T(8,128)(2,1)} %param.29) | copy-start | bytes 1572868
  7.2 8.7 %copy-start.5 = (bf16[2048,128]{1,0:T(8,128)(2,1)S(1)}, bf16[2048,128]{1,0:T(8,128)(2,1)}, u32[]{:S(2)}) copy-start(bf16[2048,128]{1,0:T(8,128)(2,1)} %param.30) | copy-start | bytes 1572868
  14.8 3.5 %copy-start.9 = (bf16[32,1,2,32]{3,2,0,1:T(2,128)(2,1)}, bf16[32,1,2,32]{3,2,0,1:T(2,128)(2,1)S(1)}, u32[]{:S(2)}) copy-start(bf16[32,1,2,32]{3,2,0,1:T(2,128)(2,1)S(1)} %get-tuple-element.148) | copy-start | bytes 12292
  16.1 2.1 copy-start.12
  32.7 11.7 %copy-start.2 = (bf16[32,2048]{1,0:T(8,128)(2,1)S(1)}, bf16[32,2048]{1,0:T(8,128)(2,1)}, u32[]{:S(2)}) copy-start(bf16[32,2048]{1,0:T(8,128)(2,1)} %param.23) | copy-start | bytes 393220
  32.7 12.6 %copy-start.14 = (bf16[2048]{0:T(1024)(128)(2,1)S(1)}, bf16[2048]{0:T(1024)(128)(2,1)}, u32[]{:S(2)}) copy-start(bf16[2048]{0:T(1024)(128)(2,1)} %param.40) | copy-start | bytes 12292
  32.7 12.6 %copy-start.13 = (f32[2048]{0:T(1024)S(1)}, f32[2048]{0:T(1024)}, u32[]{:S(2)}) copy-start(f32[2048]{0:T(1024)} %param.34) | copy-start | bytes 24580
  33.9 12.5 %copy-start.7 = (bf16[2048,44]{0,1:T(8,128)(2,1)S(1)}, bf16[2048,44]{0,1:T(8,128)(2,1)}, u32[]{:S(2)}) copy-start(bf16[2048,44]{0,1:T(8,128)(2,1)} %param.42) | copy-start | bytes 540676
  35.6 11.0 %copy-start.8 = (bf16[2048,44]{0,1:T(8,128)(2,1)S(1)}, bf16[2048,44]{0,1:T(8,128)(2,1)}, u32[]{:S(2)}) copy-start(bf16[2048,44]{0,1:T(8,128)(2,1)} %param.41) | copy-start | bytes 540676
  35.7 15.3 %copy-start.15 = (s32[32,2]{0,1:T(2,128)S(1)}, s32[32,2]{0,1:T(2,128)}, u32[]{:S(2)}) copy-start(s32[32,2]{0,1:T(2,128)} %param.35) | copy-start | bytes 772
  39.4 5.0 %all-to-all-start = ((bf16[2,32,2048]{2,1,0:T(8,128)(2,1)}), bf16[2,32,2048]{2,1,0:T(8,128)(2,1)S(1)}, u32[]{:S(2)}, u32[]{:S(2)}) async-start(bf16[2,32,2048]{2,1,0:T(8,128)(2,1)} %broadcast_in_dim.37), calls=%async_computation | async-start | bytes 524288 | tf_op jit(solution)/shard_map/all_to_all | solution.py:14
  42.8 124.9 %all-gather.2.cloned.1.call-start = ((), (), s32[]{:S(2)}) async-start(), calls=%async_computation.8 | async-start | bytes 4792320 | tf_op jit(solution)/shard_map/all_gather | solution.py:35
  47.5 5.3 %all-to-all-start.4 = ((bf16[2,2048,44]{1,2,0:T(8,128)(2,1)}), bf16[2,2048,44]{1,2,0:T(8,128)(2,1)S(1)}, u32[]{:S(2)}, u32[]{:S(2)}) async-start(bf16[2,2048,44]{1,2,0:T(8,128)(2,1)} %pad_maximum_fusion), calls=%async_computation.4 | async-start | bytes 786432 | tf_op jit(solution)/shard_map/all_to_all | solution.py:46
  51.8 0.5 copy-start.17
  54.5 74.3 %all-to-all-start.1 = ((bf16[64,4,2048]{2,1,0:T(4,128)(2,1)}), bf16[64,4,2048]{2,1,0:T(4,128)(2,1)S(1)}, u32[]{:S(2)}, u32[]{:S(2)}) async-start(bf16[64,4,2048]{2,1,0:T(4,128)(2,1)} %bitcast.26), calls=%async_computation.1 | async-start | bytes 2097152 | tf_op jit(solution)/shard_map/all_to_all | solution.py:205
  132.9 34.8 %copy-start.6 = (bf16[1,2048,88]{1,2,0:T(8,128)(2,1)S(1)}, bf16[1,2048,88]{1,2,0:T(8,128)(2,1)}, u32[]{:S(2)}) copy-start(bf16[1,2048,88]{1,2,0:T(8,128)(2,1)} %all_to_all.41) | copy-start | bytes 1081348
  172.3 7.3 %all-to-all-start.6 = ((bf16[2,2048,88]{1,2,0:T(8,128)(2,1)}), bf16[2,2048,88]{1,2,0:T(8,128)(2,1)S(1)}, u32[]{:S(2)}, u32[]{:S(2)}) async-start(bf16[2,2048,88]{1,2,0:T(8,128)(2,1)} %broadcast_in_dim.43), calls=%async_computation.6 | async-start | bytes 1441792 | tf_op jit(solution)/shard_map/all_to_all | solution.py:14
  179.6 14.3 %copy-start.20 = (bf16[88,1024]{1,0:T(8,128)(2,1)S(1)}, bf16[88,1024]{1,0:T(8,128)(2,1)}, u32[]{:S(2)}) copy-start(bf16[88,1024]{1,0:T(8,128)(2,1)} %param.43) | copy-start | bytes 540676
  180.6 5.4 %all-to-all-start.5 = ((bf16[2,2048,88]{1,2,0:T(8,128)(2,1)}), bf16[2,2048,88]{1,2,0:T(8,128)(2,1)S(1)}, u32[]{:S(2)}, u32[]{:S(2)}) async-start(bf16[2,2048,88]{1,2,0:T(8,128)(2,1)} %broadcast_in_dim.42), calls=%async_computation.5 | async-start | bytes 1441792 | tf_op jit(solution)/shard_map/all_to_all | solution.py:14
  186.0 20.1 %all-to-all-start.3 = ((bf16[64,4,1024]{2,1,0:T(4,128)(2,1)}), bf16[64,4,1024]{2,1,0:T(4,128)(2,1)S(1)}, u32[]{:S(2)}, u32[]{:S(2)}) async-start(bf16[64,4,1024]{2,1,0:T(4,128)(2,1)} %copy.120), calls=%async_computation.3 | async-start | bytes 1048576 | tf_op jit(solution)/shard_map/all_to_all | solution.py:215
  206.2 5.8 %copy-start.18 = (s32[64]{0:T(128)S(1)}, s32[64]{0:T(128)}, u32[]{:S(2)}) copy-start(s32[64]{0:T(128)} %copy-done.17) | copy-start | bytes 772
  206.2 6.0 %copy-start.10 = (bf16[32,1,2,32]{3,2,0,1:T(2,128)(2,1)S(1)}, bf16[32,1,2,32]{3,2,0,1:T(2,128)(2,1)}, u32[]{:S(2)}) copy-start(bf16[32,1,2,32]{3,2,0,1:T(2,128)(2,1)} %copy-done.9) | copy-start | bytes 12292
  206.2 6.8 %copy-start.16 = (s32[32,2]{0,1:T(2,128)S(1)}, s32[32,2]{0,1:T(2,128)}, u32[]{:S(2)}) copy-start(s32[32,2]{0,1:T(2,128)} %param.35) | copy-start | bytes 772
  206.2 6.8 %copy-start.19 = (f32[32,2]{0,1:T(2,128)S(1)}, f32[32,2]{0,1:T(2,128)}, u32[]{:S(2)}) copy-start(f32[32,2]{0,1:T(2,128)} %param.36) | copy-start | bytes 772
  206.2 58.5 %all-to-all-start.7 = ((bf16[64,32,1024]{2,1,0:T(8,128)(2,1)}), bf16[64,32,1024]{2,1,0:T(8,128)(2,1)}, u32[]{:S(2)}, u32[]{:S(2)}) async-start(bf16[64,32,1024]{2,1,0:T(8,128)(2,1)} %bitcast.180), calls=%async_computation.7 | async-start | bytes 8388608 | tf_op jit(solution)/shard_map/all_to_all | solution.py:64
  212.0 55.7 %copy-start.3 = (f32[32,2048]{1,0:T(8,128)S(1)}, f32[32,2048]{1,0:T(8,128)}, u32[]{:S(2)}) copy-start(f32[32,2048]{1,0:T(8,128)} %get-tuple-element.141) | copy-start | bytes 786436
Sparse Core Ops, SparseCore 0:
  46.5 121.1 all-gather.1
where the time goes:
time: 278 us; the launch traced here: 276 us
  waiting for transfers between devices  108 us (39%)
  starting transfers between devices  81.1 us (29%)
  matrix products  28.6 us (10%)
  local copies, waits for them, and re-layouts  20 us (7%)
  other arithmetic  18.3 us (7%)
  between operations  15.3 us (6%)
  blocking collectives  4.14 us (1%)
    all_to_all x1, starting transfers between devices, per_device(): lax.all_to_all(outgoing, 'ep', split_axis=0, concat_axis=0, tiled=True)  54.6 us
    all_to_all x1, waiting for transfers between devices, sum_at_owner(): lax.all_to_all(pieces, axis, split_axis=0, concat_axis=0, tiled=True)  51.1 us
    all_gather x1, waiting for transfers between devices, in_one_piece(): filled, at, outs = (lax.all_gather(both, axis, axis=dim, tiled=True), 0, [])  28 us
    all_to_all x1, waiting for transfers between devices, per_device(): lax.all_to_all(outgoing, 'ep', split_axis=0, concat_axis=0, tiled=True)  18.8 us
    all_to_all x3, starting transfers between devices, sent_to_all(): lax.all_to_all(jnp.broadcast_to(x[None], (size, *x.shape)), axis, 0, 0, t...  10.7 us
    all_to_all x1, waiting for transfers between devices, per_device(): lax.all_to_all(partial_value.astype(jnp.bfloat16), 'ep', split_axis=0, co...  7.86 us
    all_to_all x1, starting transfers between devices, per_device(): lax.all_to_all(partial_value.astype(jnp.bfloat16), 'ep', split_axis=0, co...  6.46 us
    dynamic_slice x2, local copies, waits for them, and re-layouts, visit(): lax.dynamic_slice_in_dim(key_cache, offset, span_len, 1)  6.41 us
  transfers between devices with their start and end apart: 8, of which 6 were waited for; matrix products, arithmetic and copies ran while one was open for 8% of the time, Pallas kernels for 0%

commit v1 on v0

--- a/solution.py
+++ b/solution.py
@@ -11,7 +11,7 @@
 
 def sent_to_all(x, axis):
     size = lax.axis_size(axis)
-    return lax.all_to_all(jnp.broadcast_to(x[None], (size, *x.shape)), axis, 0, 0, tiled=True)
+    return lax.all_gather(x, axis, axis=0)
 
 
 def taken_together(x, axis):

time: 278 us -> 267 us (0.960)
  waiting for transfers between devices: 108 us -> 96.4 us
  starting transfers between devices: 81.1 us -> 70.1 us
  other arithmetic: 18.3 us -> 23.9 us
  blocking collectives: 4.14 us -> 8.96 us
    all_to_all x3 -> x0, starting transfers between devices: 10.7 us -> none  [sent_to_all(): lax.all_to_all(jnp.broadcast_to(x[None], (size, *x.shape)), axis, 0, 0, t...]
    all_gather x0 -> x4, blocking collectives: none -> 8.96 us  [sent_to_all(): return lax.all_gather(x, axis, axis=0)]
    all_to_all x1, waiting for transfers between devices: 7.86 us -> 0.01 us  [per_device(): lax.all_to_all(partial_value.astype(jnp.bfloat16), 'ep', split_axis=0, co...]
    reduce_sum x3, other arithmetic: 1.16 us -> 6.82 us  [taken_together(): return sent_to_all(x, axis).astype(jnp.float32).sum(axis=0)]
    convert_element_type x0 -> x2, local copies, waits for them, and re-layouts: none -> 4.84 us  [taken_together(): return sent_to_all(x, axis).astype(jnp.float32).sum(axis=0)]
    all_to_all x1 -> x0, blocking collectives: 4.14 us -> none  [sent_to_all(): lax.all_to_all(jnp.broadcast_to(x[None], (size, *x.shape)), axis, 0, 0, t...]
    all_gather x1, waiting for transfers between devices: 28 us -> 24.8 us  [in_one_piece(): filled, at, outs = (lax.all_gather(both, axis, axis=dim, tiled=True), 0, [])]
  transfers between devices with their start and end apart: 8 -> 5, of which waited for: 6 -> 3; matrix products, arithmetic and copies ran while one was open for 8% -> 13% of each run, Pallas kernels for 0% -> 0%
where the time goes in v1:
time: 267 us; the launch traced here: 264 us
  waiting for transfers between devices  96.4 us (36%)
  starting transfers between devices  70.1 us (26%)
  matrix products  26.8 us (10%)
  other arithmetic  23.9 us (9%)
  local copies, waits for them, and re-layouts  22.5 us (8%)
  between operations  15.3 us (6%)
  blocking collectives  8.96 us (3%)
    all_to_all x1, starting transfers between devices, per_device(): lax.all_to_all(outgoing, 'ep', split_axis=0, concat_axis=0, tiled=True)  54.7 us
    all_to_all x1, waiting for transfers between devices, sum_at_owner(): lax.all_to_all(pieces, axis, split_axis=0, concat_axis=0, tiled=True)  52.8 us
    all_gather x1, waiting for transfers between devices, in_one_piece(): filled, at, outs = (lax.all_gather(both, axis, axis=dim, tiled=True), 0, [])  24.8 us
    all_to_all x1, waiting for transfers between devices, per_device(): lax.all_to_all(outgoing, 'ep', split_axis=0, concat_axis=0, tiled=True)  18.8 us
    all_gather x4, blocking collectives, sent_to_all(): return lax.all_gather(x, axis, axis=0)  8.96 us
    reduce_sum x3, other arithmetic, taken_together(): return sent_to_all(x, axis).astype(jnp.float32).sum(axis=0)  6.82 us
    all_to_all x1, starting transfers between devices, sum_at_owner(): lax.all_to_all(pieces, axis, split_axis=0, concat_axis=0, tiled=True)  6.82 us
    dynamic_slice x2, local copies, waits for them, and re-layouts, visit(): lax.dynamic_slice_in_dim(key_cache, offset, span_len, 1)  6.44 us
  transfers between devices with their start and end apart: 5, of which 3 were waited for; matrix products, arithmetic and copies ran while one was open for 13% of the time, Pallas kernels for 0%

profile of v1, /device:TPU:0, one launch (start us, length us, event | category | flops | bytes accessed | tf_op | source)
XLA Modules:
  0.0 264.0 jit_solution(23829418419367551)
XLA Ops:
  7.3 1.5 fusion.80
  10.5 3.2 %fusion.73 = f32[32,1024]{1,0:T(8,128)S(1)} fusion(bf16[2048,1024]{1,0:T(8,128)(2,1)} %param.28, bf16[32,2048]{1,0:T(8,128)(2,1)} %param.23, f32[2048]{0:T(1024)} %param.27, f32[32]{0:T(128)S(1)} %add_rsqrt_fusion.2), kind=kOutput, calls=%fused_computation.114 | convolution fusion | flops 134479872 | bytes 4464768 | tf_op jit(solution)/shard_map/dot_general | solution.py:120
  18.3 14.5 %while.14 = (s32[]{:T(128)}, f32[32,1,8,2]{2,3,0,1:T(2,128)}, f32[32,1,8,2]{2,3,0,1:T(2,128)}, f32[32,1,8,2,128]{4,2,3,0,1:T(8,128)}, s32[]{:T(128)}, /*index=5*...) while((s32[]{:T(128)}, f32[32,1,8,2]{2,3,0,1:T(2,128)}, ...), condition=%wide.region_5.6_spmd, body=%wide.region_2.5_spmd.sunk | while | flops 51390212 | bytes 14797119 | solution.py:174
  18.3 3.2 %constant_dynamic-slice_fusion.3 = bf16[32,256,128]{2,1,0:T(8,128)(2,1)} fusion(bf16[32,1024,128]{2,1,0:T(8,128)(2,1)} %get-tuple-element.242, s32[]{:T(128)S(6)} %select_n.26), kind=kLoop, calls=%fused_computation.22.clone.1 | loop fusion | bytes 4194308 | tf_op jit(solution)/shard_map/while/body/dynamic_slice | solution.py:150
  21.5 3.3 %copy.133 = bf16[32,256,128]{1,2,0:T(8,128)(2,1)S(1)} copy(bf16[32,256,128]{2,1,0:T(8,128)(2,1)} %constant_dynamic-slice_fusion.3) | data formatting | bytes 4194304 | tf_op jit(solution)/shard_map/while/body/dynamic_slice | solution.py:150
  25.5 1.4 fusion.104
  28.0 1.4 bitcast_add_fusion.2
  30.0 2.8 %fusion.107 = f32[32,1,8,2,128]{4,2,3,0,1:T(8,128)} fusion(bf16[32,1024,128]{2,1,0:T(8,128)(2,1)} %get-tuple-element.244, s32[]{:T(128)S(6)} %select_n.26, f32[32,1,8,2,256]{4,2,3,0,1:T(8,128)S(1)} %get-tuple-element.208, f32[32,1,8,2,128]{4,2,3,0,1:T(8,128)} %get-tuple-element.226, f32[32,8,2]{1,2,0:T(2,128)S(1)} %bitcast.186, ...), kind=kOutput, calls=%fused_computation.8.clone.1 | convolution fusion | flops 33947648 | bytes 3149828 | tf_op jit(solution)/shard_map/while/body/sgaml,slge->sgame/dot_general | solution.py:166
  35.8 3.0 %convolution_convert_fusion.1 = bf16[32,2048]{1,0:T(8,128)(2,1)S(1)} fusion(bf16[1024,2048]{1,0:T(8,128)(2,1)} %param.33, f32[4,8,8,128]{3,2,1,0:T(8,128)S(1)} %bitcast.194, f32[4,8,8,128]{3,2,1,0:T(8,128)S(1)} %bitcast.196, f32[4,8,8,128]{3,2,1,0:T(8,128)S(1)} %bitcast.195, f32[1024]{0:T(1024)S(1)} %get-tuple-element.144, f32[1024]{0:T(1024)S(1)} %get-tuple-element.145), kind=kOutput, calls=%fused_computation.32 | convolution fusion | flops 134447104 | bytes 4726784 | tf_op jit(solution)/shard_map/dot_general | solution.py:180
  38.8 2.0 all-gather
  43.9 3.5 %all-to-all-start.2 = ((bf16[2,2048,44]{1,2,0:T(8,128)(2,1)}), bf16[2,2048,44]{1,2,0:T(8,128)(2,1)S(1)}, u32[]{:S(2)}, u32[]{:S(2)}) async-start(bf16[2,2048,44]{1,2,0:T(8,128)(2,1)} %pad_maximum_fusion), calls=%async_computation.2 | async-start | bytes 786432 | tf_op jit(solution)/shard_map/all_to_all | solution.py:46
  49.2 1.6 broadcast_in_dim.26
  50.8 54.7 %all-to-all-start = ((bf16[64,4,2048]{2,1,0:T(4,128)(2,1)}), bf16[64,4,2048]{2,1,0:T(4,128)(2,1)S(1)}, u32[]{:S(2)}, u32[]{:S(2)}) async-start(bf16[64,4,2048]{2,1,0:T(4,128)(2,1)} %bitcast.27), calls=%async_computation | async-start | bytes 2097152 | tf_op jit(solution)/shard_map/all_to_all | solution.py:205
  106.3 18.8 %all-to-all-done = bf16[64,4,2048]{2,1,0:T(4,128)(2,1)S(1)} async-done(((bf16[64,4,2048]{2,1,0:T(4,128)(2,1)}), bf16[64,4,2048]{2,1,0:T(4,128)(2,1)S(1)}, u32[]{:S(2)}, u32[]{:S(2)}) %all-to-all-start) | async-done | bytes 1048608 | tf_op jit(solution)/shard_map/all_to_all | solution.py:205
  125.4 1.9 fusion.34
  127.4 1.9 fusion.42
  129.3 2.2 all-gather.1
  134.5 5.1 %all-to-all-start.1 = ((bf16[64,4,1024]{2,1,0:T(4,128)(2,1)}), bf16[64,4,1024]{2,1,0:T(4,128)(2,1)S(1)}, u32[]{:S(2)}, u32[]{:S(2)}) async-start(bf16[64,4,1024]{2,1,0:T(4,128)(2,1)} %copy.101), calls=%async_computation.1 | async-start | bytes 1048576 | tf_op jit(solution)/shard_map/all_to_all | solution.py:215
  139.6 24.8 %all-gather.6.cloned.1.call-done = bf16[2048,1025]{1,0:T(8,128)(2,1)} async-done(((bf16[32,1025]{1,0:T(8,128)(2,1)}), bf16[2048,1025]{1,0:T(8,128)(2,1)}) %all-gather.6.cloned.1.call-update) | async-done | bytes 4198416 | tf_op jit(solution)/shard_map/all_gather | solution.py:35
  164.4 3.7 %fusion.27 = bf16[2048,88]{0,1:T(8,128)(2,1)S(1)} fusion(bf16[2048,1025]{1,0:T(8,128)(2,1)} %all-gather.6.cloned.1.call-done, bf16[1,2048,88]{1,2,0:T(8,128)(2,1)S(1)} %copy-done.6), kind=kOutput, calls=%fused_computation.31 | convolution fusion | flops 369278976 | bytes 4734976 | tf_op jit(solution)/shard_map/dot_general | solution.py:248
  168.1 2.3 all-gather.3
  170.5 1.4 fusion.24
  171.9 2.5 all-gather.2
  174.3 2.4 reshape.329
  176.7 2.4 reshape.328
  179.2 4.0 %reduce_sum.115 = f32[2048,88]{0,1:T(8,128)} reduce(f32[2,2048,88]{1,0,2:T(2,128)} %reshape.329, f32[]{:T(128)} %constant.41.clone.1), dimensions={0}, to_apply=%region_14.15 | reduce | flops 180224 | bytes 2162692 | tf_op jit(solution)/shard_map/reduce_sum | solution.py:18
  183.1 2.8 %reduce_sum.114 = f32[2048,88]{0,1:T(8,128)} reduce(f32[2,2048,88]{1,0,2:T(2,128)S(1)} %reshape.328, f32[]{:T(128)} %constant.41.clone.1), dimensions={0}, to_apply=%region_13.14 | reduce | flops 180224 | bytes 2162692 | tf_op jit(solution)/shard_map/reduce_sum | solution.py:18
  185.9 1.3 convert_reduce_fusion.2
  187.2 4.6 %multiply_convert_fusion = bf16[2048,1024]{1,0:T(8,128)(2,1)} fusion(bf16[88,1024]{1,0:T(8,128)(2,1)} %param.43, f32[2048]{0:T(1024)S(1)} %convert_reduce_fusion.2, f32[2048,88]{0,1:T(8,128)} %reduce_sum.115, f32[2048,88]{0,1:T(8,128)} %reduce_sum.114), kind=kOutput, calls=%fused_computation.24 | convolution fusion | flops 374374400 | bytes 5824512 | tf_op jit(solution)/shard_map/dot_general | solution.py:256
  191.9 6.8 %all-to-all-start.3 = ((bf16[64,32,1024]{2,1,0:T(8,128)(2,1)}), bf16[64,32,1024]{2,1,0:T(8,128)(2,1)}, u32[]{:S(2)}, u32[]{:S(2)}) async-start(bf16[64,32,1024]{2,1,0:T(8,128)(2,1)} %bitcast.187), calls=%async_computation.3 | async-start | bytes 8388608 | tf_op jit(solution)/shard_map/all_to_all | solution.py:64
  200.3 52.8 %all-to-all-done.3 = bf16[64,32,1024]{2,1,0:T(8,128)(2,1)} async-done(((bf16[64,32,1024]{2,1,0:T(8,128)(2,1)}), bf16[64,32,1024]{2,1,0:T(8,128)(2,1)}, u32[]{:S(2)}, u32[]{:S(2)}) %all-to-all-start.3) | async-done | bytes 4194336 | tf_op jit(solution)/shard_map/all_to_all | solution.py:64
  253.0 3.0 %convert_reduce_fusion = f32[32,1024]{1,0:T(8,128)S(1)} fusion(bf16[64,32,1024]{2,1,0:T(8,128)(2,1)} %all-to-all-done.3), kind=kLoop, calls=%fused_computation.23 | loop fusion | flops 4161536 | bytes 4325376 | tf_op jit(solution)/shard_map/reduce_sum | solution.py:65
  (114 shorter events, 22.5 us)
Async XLA Ops:
  7.2 125.5 %copy-start = (bf16[1,704,1024]{2,1,0:T(8,128)(2,1)S(1)}, bf16[1,704,1024]{2,1,0:T(8,128)(2,1)}, u32[]{:S(2)}) copy-start(bf16[1,704,1024]{2,1,0:T(8,128)(2,1)} %param.39) | copy-start | bytes 4325380
  7.2 7.0 %copy-start.1 = (bf16[32,2048]{1,0:T(8,128)(2,1)S(1)}, bf16[32,2048]{1,0:T(8,128)(2,1)}, u32[]{:S(2)}) copy-start(bf16[32,2048]{1,0:T(8,128)(2,1)} %param.23) | copy-start | bytes 393220
  7.2 7.0 %copy-start.11 = (f32[2048]{0:T(1024)S(1)}, f32[2048]{0:T(1024)}, u32[]{:S(2)}) copy-start(f32[2048]{0:T(1024)} %param.27) | copy-start | bytes 24580
  7.2 7.0 %copy-start.4 = (bf16[2048,128]{1,0:T(8,128)(2,1)S(1)}, bf16[2048,128]{1,0:T(8,128)(2,1)}, u32[]{:S(2)}) copy-start(bf16[2048,128]{1,0:T(8,128)(2,1)} %param.29) | copy-start | bytes 1572868
  7.2 8.7 %copy-start.5 = (bf16[2048,128]{1,0:T(8,128)(2,1)S(1)}, bf16[2048,128]{1,0:T(8,128)(2,1)}, u32[]{:S(2)}) copy-start(bf16[2048,128]{1,0:T(8,128)(2,1)} %param.30) | copy-start | bytes 1572868
  7.2 157.2 %all-gather.6.cloned.1.call-start = ((), (), s32[]{:S(2)}) async-start(), calls=%async_computation.4 | async-start | bytes 4792320 | tf_op jit(solution)/shard_map/all_gather | solution.py:35
  14.8 3.5 %copy-start.9 = (bf16[32,1,2,32]{3,2,0,1:T(2,128)(2,1)}, bf16[32,1,2,32]{3,2,0,1:T(2,128)(2,1)S(1)}, u32[]{:S(2)}) copy-start(bf16[32,1,2,32]{3,2,0,1:T(2,128)(2,1)S(1)} %get-tuple-element.139) | copy-start | bytes 12292
  16.2 2.1 copy-start.13
  32.8 8.0 %copy-start.2 = (bf16[32,2048]{1,0:T(8,128)(2,1)S(1)}, bf16[32,2048]{1,0:T(8,128)(2,1)}, u32[]{:S(2)}) copy-start(bf16[32,2048]{1,0:T(8,128)(2,1)} %param.23) | copy-start | bytes 393220
  32.8 8.9 %copy-start.15 = (bf16[2048]{0:T(1024)(128)(2,1)S(1)}, bf16[2048]{0:T(1024)(128)(2,1)}, u32[]{:S(2)}) copy-start(bf16[2048]{0:T(1024)(128)(2,1)} %param.40) | copy-start | bytes 12292
  32.8 8.9 %copy-start.14 = (f32[2048]{0:T(1024)S(1)}, f32[2048]{0:T(1024)}, u32[]{:S(2)}) copy-start(f32[2048]{0:T(1024)} %param.34) | copy-start | bytes 24580
  32.8 9.9 %copy-start.7 = (bf16[2048,44]{0,1:T(8,128)(2,1)S(1)}, bf16[2048,44]{0,1:T(8,128)(2,1)}, u32[]{:S(2)}) copy-start(bf16[2048,44]{0,1:T(8,128)(2,1)} %param.42) | copy-start | bytes 540676
  34.0 8.9 %copy-start.8 = (bf16[2048,44]{0,1:T(8,128)(2,1)S(1)}, bf16[2048,44]{0,1:T(8,128)(2,1)}, u32[]{:S(2)}) copy-start(bf16[2048,44]{0,1:T(8,128)(2,1)} %param.41) | copy-start | bytes 540676
  35.8 11.6 %copy-start.16 = (s32[32,2]{0,1:T(2,128)S(1)}, s32[32,2]{0,1:T(2,128)}, u32[]{:S(2)}) copy-start(s32[32,2]{0,1:T(2,128)} %param.35) | copy-start | bytes 772
  43.9 5.3 %all-to-all-start.2 = ((bf16[2,2048,44]{1,2,0:T(8,128)(2,1)}), bf16[2,2048,44]{1,2,0:T(8,128)(2,1)S(1)}, u32[]{:S(2)}, u32[]{:S(2)}) async-start(bf16[2,2048,44]{1,2,0:T(8,128)(2,1)} %pad_maximum_fusion), calls=%async_computation.2 | async-start | bytes 786432 | tf_op jit(solution)/shard_map/all_to_all | solution.py:46
  48.2 0.5 copy-start.18
  50.8 74.4 %all-to-all-start = ((bf16[64,4,2048]{2,1,0:T(4,128)(2,1)}), bf16[64,4,2048]{2,1,0:T(4,128)(2,1)S(1)}, u32[]{:S(2)}, u32[]{:S(2)}) async-start(bf16[64,4,2048]{2,1,0:T(4,128)(2,1)} %bitcast.27), calls=%async_computation | async-start | bytes 2097152 | tf_op jit(solution)/shard_map/all_to_all | solution.py:205
  129.3 35.1 %copy-start.6 = (bf16[1,2048,88]{1,2,0:T(8,128)(2,1)S(1)}, bf16[1,2048,88]{1,2,0:T(8,128)(2,1)}, u32[]{:S(2)}) copy-start(bf16[1,2048,88]{1,2,0:T(8,128)(2,1)} %all_to_all.27) | copy-start | bytes 1081348
  134.5 57.3 %all-to-all-start.1 = ((bf16[64,4,1024]{2,1,0:T(4,128)(2,1)}), bf16[64,4,1024]{2,1,0:T(4,128)(2,1)S(1)}, u32[]{:S(2)}, u32[]{:S(2)}) async-start(bf16[64,4,1024]{2,1,0:T(4,128)(2,1)} %copy.101), calls=%async_computation.1 | async-start | bytes 1048576 | tf_op jit(solution)/shard_map/all_to_all | solution.py:215
  164.4 6.1 %copy-start.12 = (bf16[2048,1025]{1,0:T(8,128)(2,1)S(1)}, bf16[2048,1025]{1,0:T(8,128)(2,1)}, u32[]{:S(2)}) copy-start(bf16[2048,1025]{1,0:T(8,128)(2,1)} %all-gather.6.cloned.1.call-done) | copy-start | bytes 12595204
  191.8 6.9 %copy-start.19 = (s32[64]{0:T(128)S(1)}, s32[64]{0:T(128)}, u32[]{:S(2)}) copy-start(s32[64]{0:T(128)} %copy-done.18) | copy-start | bytes 772
  191.8 7.1 %copy-start.10 = (bf16[32,1,2,32]{3,2,0,1:T(2,128)(2,1)S(1)}, bf16[32,1,2,32]{3,2,0,1:T(2,128)(2,1)}, u32[]{:S(2)}) copy-start(bf16[32,1,2,32]{3,2,0,1:T(2,128)(2,1)} %copy-done.9) | copy-start | bytes 12292
  191.8 7.8 %copy-start.17 = (s32[32,2]{0,1:T(2,128)S(1)}, s32[32,2]{0,1:T(2,128)}, u32[]{:S(2)}) copy-start(s32[32,2]{0,1:T(2,128)} %param.35) | copy-start | bytes 772
  191.9 7.8 %copy-start.20 = (f32[32,2]{0,1:T(2,128)S(1)}, f32[32,2]{0,1:T(2,128)}, u32[]{:S(2)}) copy-start(f32[32,2]{0,1:T(2,128)} %param.36) | copy-start | bytes 772
  191.9 61.2 %all-to-all-start.3 = ((bf16[64,32,1024]{2,1,0:T(8,128)(2,1)}), bf16[64,32,1024]{2,1,0:T(8,128)(2,1)}, u32[]{:S(2)}, u32[]{:S(2)}) async-start(bf16[64,32,1024]{2,1,0:T(8,128)(2,1)} %bitcast.187), calls=%async_computation.3 | async-start | bytes 8388608 | tf_op jit(solution)/shard_map/all_to_all | solution.py:64
  198.7 57.4 %copy-start.3 = (f32[32,2048]{1,0:T(8,128)S(1)}, f32[32,2048]{1,0:T(8,128)}, u32[]{:S(2)}) copy-start(f32[32,2048]{1,0:T(8,128)} %get-tuple-element.132) | copy-start | bytes 786436
Sparse Core Ops, SparseCore 0:
  42.9 121.4 all-gather.5
